TPU v7x, 32 devices: a whole 2x2x4 slice. The times are simulated.
32 devices in a mesh: rep: 2 (over x), fs: 8 (over z, y), tp: 2 (over core).
Axes of the slice: x: 2, y: 2, z: 4, core: 2. Of those that a mesh axis runs over, the one named last changes fastest.
Arguments:
- tokens: bfloat16 [12288, 2048], P(('rep', 'fs'), 'tp'), may hold values from -6 to 6
- first_norm_gain: bfloat16 [2048], replicated, may hold values from 0.099609375 to 1.8984375
- query_projection_weight: bfloat16 [2048, 512], P('fs', 'tp'), may hold values from -0.125 to 0.125
- key_projection_weight: bfloat16 [2048, 512], P('fs', 'tp'), may hold values from -0.125 to 0.125
- value_projection_weight: bfloat16 [2048, 1024], P('fs', 'tp'), may hold values from -0.125 to 0.125
- output_gate_weight: bfloat16 [2048, 1024], P('fs', 'tp'), may hold values from -0.125 to 0.125
- decay_projection_weight: bfloat16 [2048, 512], P('fs', 'tp'), may hold values from -0.375 to 0.375
- fading_shift_vector: float32 [512], P('tp'), may hold values from -1 to 4
- added_fading_exponent: float32 [12288, 512], P(('rep', 'fs'), 'tp'), may hold values from -0.7 to 0
- per_head_gain: bfloat16 [128], replicated, may hold values from 0.099609375 to 1.8984375
- mixer_result_matrix: bfloat16 [1024, 2048], P('tp', 'fs'), may hold values from -0.1875 to 0.1875
- second_norm_gain: bfloat16 [2048], replicated, may hold values from 0.099609375 to 1.8984375
- up_linear_weight: bfloat16 [2048, 3072], P('fs', 'tp'), may hold values from -0.125 to 0.125
- up_gating_weight: bfloat16 [2048, 3072], P('fs', 'tp'), may hold values from -0.125 to 0.125
- depthwise_taps: bfloat16 [2, 3, 3072], P(None, None, 'tp'), may hold values from -3.5 to 3.5
- depthwise_bias: bfloat16 [2, 3072], P(None, 'tp'), may hold values from -3 to 3
- down_projection_weight: bfloat16 [3072, 2048], P('tp', 'fs'), may hold values from -0.109375 to 0.109375
Outputs:
- mixed: bfloat16 [12288, 2048], P(('rep', 'fs'), 'tp')
All inputs are finite; a program needn't handle non-finite values.
Results may differ from a plain program's by a relative error of at most 0.018.
Values may be sent and summed in bfloat16 or wider, within the bound.
A program may use at most 128 MiB of HBM per device.

v0:
```python
import jax
import jax.numpy as jnp
from jax import lax
from jax.sharding import PartitionSpec as P

KEY_DIM = 64
VALUE_DIM = 128
BLOCK = 64
SEQ_LEN = 256
norm_eps = 1e-06
fading_sharpness = 16.0


def normalize(source, gain):
    widened = source.astype(jnp.float32)
    scaled = widened * lax.rsqrt(jnp.mean(widened * widened, axis=-1, keepdims=True) + norm_eps)
    return (scaled * gain.astype(jnp.float32)).astype(jnp.bfloat16)


def direction(queries, key_heads, value_heads, fading_exponent):
    sequences, length, head_count, key_depth = queries.shape
    value_depth = value_heads.shape[-1]
    block_count = length // BLOCK
    query_blocks = queries.reshape(sequences, block_count, BLOCK, head_count, key_depth)
    key_blocks = key_heads.reshape(sequences, block_count, BLOCK, head_count, key_depth)
    value_blocks = value_heads.reshape(sequences, block_count, BLOCK, head_count, value_depth)
    cumulative = jnp.cumsum(
        fading_exponent.reshape(sequences, block_count, BLOCK, head_count, key_depth), axis=2
    )
    block_total = cumulative[:, :, -1:]
    query_decayed = query_blocks * jnp.exp(cumulative)
    key_inverse = key_blocks * jnp.exp(-cumulative)
    key_carried = key_blocks * jnp.exp(block_total - cumulative)
    lower_mask = jnp.tril(jnp.ones((BLOCK, BLOCK), dtype=bool))
    scores = jnp.einsum(
        "snihd,snjhd->snhij", query_decayed, key_inverse, precision=lax.Precision.HIGHEST
    )
    scores = jnp.where(lower_mask, scores, 0.0)
    within_block = jnp.einsum(
        "snhij,snjhv->snihv", scores, value_blocks, precision=lax.Precision.HIGHEST
    )
    increments = jnp.einsum(
        "snchd,snchv->nshdv", key_carried, value_blocks, precision=lax.Precision.HIGHEST
    )
    carry_decay = jnp.moveaxis(jnp.exp(block_total[:, :, 0]), 1, 0)

    def advance(running, inputs):
        factor, update = inputs
        return (factor[..., None] * running + update, running)

    initial = jnp.zeros((sequences, head_count, key_depth, value_depth), jnp.float32)
    unused, previous = lax.scan(advance, initial, (carry_decay, increments))
    across_blocks = jnp.einsum(
        "snchd,nshdv->snchv", query_decayed, previous, precision=lax.Precision.HIGHEST
    )
    return (within_block + across_blocks).reshape(sequences, length, head_count, value_depth)


def mixer_heads(queries_raw, keys_raw, values_raw, gates_raw, fading_exponent, per_head_gain):
    row_count = queries_raw.shape[0]
    head_count = values_raw.shape[1] // VALUE_DIM
    key_shape = (row_count // SEQ_LEN, SEQ_LEN, head_count, KEY_DIM)
    value_shape = (row_count // SEQ_LEN, SEQ_LEN, head_count, VALUE_DIM)
    queries = queries_raw.astype(jnp.float32).reshape(key_shape) * KEY_DIM ** (-0.5)
    key_heads = keys_raw.astype(jnp.float32).reshape(key_shape)
    value_heads = values_raw.astype(jnp.float32).reshape(value_shape)
    decay_heads = fading_exponent.reshape(key_shape)
    forward = direction(queries, key_heads, value_heads, decay_heads)
    backward = direction(
        jnp.flip(queries, 1),
        jnp.flip(key_heads, 1),
        jnp.flip(value_heads, 1),
        jnp.flip(decay_heads, 1),
    )
    attention = forward + jnp.flip(backward, 1)
    scaled = attention * lax.rsqrt(
        jnp.mean(attention * attention, axis=-1, keepdims=True) + norm_eps
    )
    scaled = scaled * per_head_gain.astype(jnp.float32)
    merged = scaled.reshape(row_count, head_count * VALUE_DIM)
    return (merged * jax.nn.silu(gates_raw.astype(jnp.float32))).astype(jnp.bfloat16)


def depthwise(linear_out, gated_out, depthwise_taps, depthwise_bias):
    row_count, channels = linear_out.shape

    def smooth(source, taps, offset_bias):
        framed = source.astype(jnp.float32).reshape(row_count // SEQ_LEN, SEQ_LEN, channels)
        tap_count = taps.shape[0]
        leading_zero_fill = tap_count // 2
        padded = jnp.pad(
            framed, ((0, 0), (leading_zero_fill, tap_count - 1 - leading_zero_fill), (0, 0))
        )
        result = offset_bias.astype(jnp.float32)
        for shift_index in range(tap_count):
            result = result + padded[:, shift_index : shift_index + SEQ_LEN] * taps[
                shift_index
            ].astype(jnp.float32)
        return result

    linear_conv = smooth(linear_out, depthwise_taps[0], depthwise_bias[0])
    gate_conv = smooth(gated_out, depthwise_taps[1], depthwise_bias[1])
    return (linear_conv * jax.nn.silu(gate_conv)).astype(jnp.bfloat16).reshape(row_count, channels)


def fold_rows(source, weight_pieces):
    return tuple(
        (
            jnp.dot(source, weight_piece, preferred_element_type=jnp.float32)
            for weight_piece in weight_pieces
        )
    )


def emit_with(source, weight_piece):
    return jnp.dot(source, weight_piece, preferred_element_type=jnp.float32)


def local(
    tokens,
    first_norm_gain,
    query_projection_weight,
    key_projection_weight,
    value_projection_weight,
    output_gate_weight,
    decay_projection_weight,
    fading_shift_vector,
    added_fading_exponent,
    per_head_gain,
    mixer_result_matrix,
    second_norm_gain,
    up_linear_weight,
    up_gating_weight,
    depthwise_taps,
    depthwise_bias,
    down_projection_weight,
):
    whole_rows = lax.all_gather(tokens, "tp", axis=1, tiled=True)
    normed = normalize(whole_rows, first_norm_gain)
    mapped_token_matrix = fold_rows(
        normed,
        (
            lax.all_gather(query_projection_weight, "fs", axis=0, tiled=True),
            lax.all_gather(key_projection_weight, "fs", axis=0, tiled=True),
            lax.all_gather(value_projection_weight, "fs", axis=0, tiled=True),
            lax.all_gather(output_gate_weight, "fs", axis=0, tiled=True),
            lax.all_gather(decay_projection_weight, "fs", axis=0, tiled=True),
        ),
    )
    queries_raw = mapped_token_matrix[0].astype(jnp.bfloat16)
    keys_raw = mapped_token_matrix[1].astype(jnp.bfloat16)
    values_raw = mapped_token_matrix[2].astype(jnp.bfloat16)
    gates_raw = mapped_token_matrix[3].astype(jnp.bfloat16)
    fading_exponent = (
        jax.nn.log_sigmoid(mapped_token_matrix[4] + fading_shift_vector) / fading_sharpness
        + added_fading_exponent
    )
    mixed_heads = mixer_heads(
        queries_raw, keys_raw, values_raw, gates_raw, fading_exponent, per_head_gain
    )
    mixer_terms = emit_with(
        mixed_heads, lax.all_gather(mixer_result_matrix, "fs", axis=1, tiled=True)
    )
    feature_share = tokens.shape[1]
    summed = lax.psum(mixer_terms.astype(jnp.bfloat16), "tp").astype(jnp.float32)
    full_after = (whole_rows.astype(jnp.float32) + summed).astype(jnp.bfloat16)
    after_mixer = lax.dynamic_slice_in_dim(
        full_after, lax.axis_index("tp") * feature_share, feature_share, 1
    )
    normed_two = normalize(full_after, second_norm_gain)
    upward = fold_rows(
        normed_two,
        (
            lax.all_gather(up_linear_weight, "fs", axis=0, tiled=True),
            lax.all_gather(up_gating_weight, "fs", axis=0, tiled=True),
        ),
    )
    linear_out = upward[0].astype(jnp.bfloat16)
    gated_out = upward[1].astype(jnp.bfloat16)
    hidden = depthwise(linear_out, gated_out, depthwise_taps, depthwise_bias)
    channel_terms = emit_with(
        hidden, lax.all_gather(down_projection_weight, "fs", axis=1, tiled=True)
    )
    channel_part = lax.psum_scatter(
        channel_terms.astype(jnp.bfloat16), "tp", scatter_dimension=1, tiled=True
    ).astype(jnp.float32)
    return (after_mixer.astype(jnp.float32) + channel_part).astype(jnp.bfloat16)


def solution(mesh):
    return jax.shard_map(
        local,
        mesh=mesh,
        in_specs=(
            P(("rep", "fs"), "tp"),
            P(),
            P("fs", "tp"),
            P("fs", "tp"),
            P("fs", "tp"),
            P("fs", "tp"),
            P("fs", "tp"),
            P("tp"),
            P(("rep", "fs"), "tp"),
            P(),
            P("tp", "fs"),
            P(),
            P("fs", "tp"),
            P("fs", "tp"),
            P(None, None, "tp"),
            P(None, "tp"),
            P("tp", "fs"),
        ),
        out_specs=P(("rep", "fs"), "tp"),
        check_vma=False,
    )
```

profile of v0, /device:TPU:0, one launch (start us, length us, event | category | flops | bytes accessed | tf_op | source)
XLA Modules:
  0.0 659.0 jit_solution(8518647654533081212)
XLA Ops:
  11.8 11.9 %all-gather.11.cloned.1.call-done = bf16[768,2048]{1,0:T(8,128)(2,1)} async-done(((bf16[768,1024]{1,0:T(8,128)(2,1)}), bf16[768,2048]{1,0:T(8,128)(2,1)}) %all-gather.11.cloned.1.call-update) | async-done | bytes 3145744 | tf_op jit(solution)/shard_map/all_gather | solution.py:138
  26.3 41.0 %all-gather.17.cloned.1.call-done = bf16[2048,256]{1,0:T(8,128)(2,1)} async-done(((bf16[256,256]{1,0:T(8,128)(2,1)}), bf16[2048,256]{1,0:T(8,128)(2,1)}) %all-gather.17.cloned.1.call-update) | async-done | bytes 1048592 | tf_op jit(solution)/shard_map/all_gather | solution.py:147
  73.4 35.2 %all-gather.19.cloned.1.call-done = bf16[2048,256]{1,0:T(8,128)(2,1)} async-done(((bf16[256,256]{1,0:T(8,128)(2,1)}), bf16[2048,256]{1,0:T(8,128)(2,1)}) %all-gather.19.cloned.1.call-update) | async-done | bytes 1048592 | tf_op jit(solution)/shard_map/all_gather | solution.py:144
  119.4 30.1 %all-gather.15.cloned.1.call-done = bf16[2048,256]{1,0:T(8,128)(2,1)} async-done(((bf16[256,256]{1,0:T(8,128)(2,1)}), bf16[2048,256]{1,0:T(8,128)(2,1)}) %all-gather.15.cloned.1.call-update) | async-done | bytes 1048592 | tf_op jit(solution)/shard_map/all_gather | solution.py:143
  161.5 4.8 exponential_multiply_fusion.3
  177.7 21.6 %all-gather.13.cloned.1.call-done = bf16[2048,512]{1,0:T(8,128)(2,1)} async-done(((bf16[256,512]{1,0:T(8,128)(2,1)}), bf16[2048,512]{1,0:T(8,128)(2,1)}) %all-gather.13.cloned.1.call-update) | async-done | bytes 2097168 | tf_op jit(solution)/shard_map/all_gather | solution.py:145
  199.3 5.3 convolution_convert_fusion.5
  214.6 8.1 %while.26 = (s32[]{:T(128)}, f32[3,4,64,128]{3,2,1,0:T(8,128)S(1)}, f32[4,3,4,64,128]{4,3,2,0,1:T(8,128)}, f32[4,3,4,64]{3,2,0,1:T(4,128)S(1)}, f32[4,3,4,64,128]{4,3,2,1,0:T(8,128)}, /*index=5*/s32[]{:T(128)}, s32[]{:T(128)}) while((s32[]{:T(128)}, f32[3,4,64,128]{3,2,1,0:T(8,128)S(1)}, f32[4,3,4,64,128]{4,3,2,0,1:T(8,128)}, ...), condition=%wide.region_3.4_spmd.clone, body=%wide.region_2.3_spmd.clone.sunk | while | flops 393219 | bytes 1975904 | solution.py:52
  229.7 10.2 %rev.17 = f32[3,256,4,128]{3,1,2,0:T(8,128)S(1)} reverse(f32[3,256,4,128]{3,1,2,0:T(8,128)} %copy.79), dimensions={1} | reverse | bytes 3145728 | tf_op jit(solution)/shard_map/jit(_flip)/rev | solution.py:72
  239.9 5.3 fusion.11
  246.5 10.9 %while.27 = (s32[]{:T(128)}, f32[3,4,64,128]{3,2,1,0:T(8,128)S(1)}, f32[4,3,4,64,128]{4,3,2,0,1:T(8,128)}, f32[4,3,4,64]{3,2,0,1:T(4,128)}, f32[4,3,4,64,128]{4,3,2,1,0:T(8,128)}, /*index=5*/s32[]{:T(128)}, s32[]{:T(128)}) while((s32[]{:T(128)}, f32[3,4,64,128]{3,2,1,0:T(8,128)S(1)}, f32[4,3,4,64,128]{4,3,2,0,1:T(8,128)}, ...), condition=%wide.region_6.7_spmd.clone, body=%wide.region_5.6_spmd.clone.sunk | while | flops 393219 | bytes 1975904 | solution.py:52
  264.1 10.6 %rev.21 = f32[3,256,4,128]{3,1,2,0:T(8,128)S(1)} reverse(f32[3,256,4,128]{3,1,2,0:T(8,128)} %bitcast.93), dimensions={1} | reverse | bytes 3145728 | tf_op jit(solution)/shard_map/jit(_flip)/rev | solution.py:75
  277.9 22.0 %all-gather.23.cloned.1.call-done = bf16[512,2048]{1,0:T(8,128)(2,1)} async-done(((bf16[512,256]{1,0:T(8,128)(2,1)}), bf16[512,2048]{1,0:T(8,128)(2,1)}) %all-gather.23.cloned.1.call-update) | async-done | bytes 2097168 | tf_op jit(solution)/shard_map/all_gather | solution.py:162
  299.9 8.1 %convolution_convert_fusion = bf16[768,2048]{1,0:T(8,128)(2,1)} fusion(bf16[512,2048]{1,0:T(8,128)(2,1)} %all-gather.23.cloned.1.call-done, f32[96,8,4,128]{3,2,1,0:T(4,128)} %bitcast.99, bf16[2048,512]{1,0:T(8,128)(2,1)} %all-gather.21.cloned.1.call-done, bf16[768,2048]{1,0:T(8,128)(2,1)S(1)} %copy-done.2, f32[2048]{0:T(1024)S(1)} %convert_element_type.115, ...), kind=kOutput, calls=%fused_computation.19 | convolution fusion | flops 3232235520 | bytes 12069888 | tf_op jit(solution)/shard_map/dot_general | solution.py:116
  310.3 19.3 %all-reduce.4.cloned.1.call-done = bf16[768,2048]{1,0:T(8,128)(2,1)} async-done(((bf16[768,2048]{1,0:T(8,128)(2,1)}), bf16[768,2048]{1,0:T(8,128)(2,1)}) %all-reduce.4.cloned.1.call-update) | async-done | bytes 3145744 | tf_op jit(solution)/shard_map/psum | solution.py:165
  329.6 5.1 fusion
  334.7 97.0 %all-gather.25.cloned.1.call-done = bf16[2048,1536]{1,0:T(8,128)(2,1)} async-done(((bf16[256,1536]{1,0:T(8,128)(2,1)}), bf16[2048,1536]{1,0:T(8,128)(2,1)}) %all-gather.25.cloned.1.call-update) | async-done | bytes 6291472 | tf_op jit(solution)/shard_map/all_gather | solution.py:174
  431.7 8.9 %convolution_convert_fusion.2 = bf16[768,1536]{1,0:T(8,128)(2,1)S(1)} fusion(bf16[2048,1536]{1,0:T(8,128)(2,1)} %all-gather.25.cloned.1.call-done, bf16[768,2048]{1,0:T(8,128)(2,1)} %get-tuple-element.166, f32[2048]{0:T(1024)S(1)} %convert_element_type.133, f32[768]{0:T(1024)S(1)} %add_rsqrt_fusion.1), kind=kOutput, calls=%fused_computation.21 | convolution fusion | flops 4839309312 | bytes 11807744 | tf_op jit(solution)/shard_map/dot_general | solution.py:109
  443.5 87.2 %all-gather.27.cloned.1.call-done = bf16[2048,1536]{1,0:T(8,128)(2,1)} async-done(((bf16[256,1536]{1,0:T(8,128)(2,1)}), bf16[2048,1536]{1,0:T(8,128)(2,1)}) %all-gather.27.cloned.1.call-update) | async-done | bytes 6291472 | tf_op jit(solution)/shard_map/all_gather | solution.py:175
  530.7 8.2 %convolution_convert_fusion.1 = bf16[768,1536]{1,0:T(8,128)(2,1)S(1)} fusion(bf16[2048,1536]{1,0:T(8,128)(2,1)} %all-gather.27.cloned.1.call-done, bf16[768,2048]{1,0:T(8,128)(2,1)S(1)} %copy-done.3, f32[2048]{0:T(1024)S(1)} %convert_element_type.133, f32[768]{0:T(1024)S(1)} %add_rsqrt_fusion.1), kind=kOutput, calls=%fused_computation.20 | convolution fusion | flops 4839309312 | bytes 11807744 | tf_op jit(solution)/shard_map/dot_general | solution.py:109
  541.4 5.3 multiply_convert_fusion
  546.7 83.7 %all-gather.29.cloned.1.call-done = bf16[1536,2048]{1,0:T(8,128)(2,1)} async-done(((bf16[1536,256]{1,0:T(8,128)(2,1)}), bf16[1536,2048]{1,0:T(8,128)(2,1)}) %all-gather.29.cloned.1.call-update) | async-done | bytes 6291472 | tf_op jit(solution)/shard_map/all_gather | solution.py:182
  630.4 9.0 %convolution_convert_fusion.3 = bf16[768,2048]{1,0:T(8,128)(2,1)} fusion(bf16[768,1536]{1,0:T(8,128)(2,1)} %bitcast.98, bf16[1536,2048]{1,0:T(8,128)(2,1)} %all-gather.29.cloned.1.call-done), kind=kOutput, calls=%fused_computation.22 | convolution fusion | flops 4833411072 | bytes 11796480 | tf_op jit(solution)/shard_map/dot_general | solution.py:116
  639.5 9.3 %reduce-scatter.2.cloned.1.call-done = bf16[768,1024]{1,0:T(8,128)(2,1)} async-done(((bf16[768,2048]{1,0:T(8,128)(2,1)}), bf16[768,1024]{1,0:T(8,128)(2,1)}) %reduce-scatter.2.cloned.1.call-update) | async-done | bytes 1572880 | tf_op jit(solution)/shard_map/reduce_scatter | solution.py:184
  (153 shorter events, 105.5 us)
Async XLA Ops:
  6.5 4.8 copy-start.15
  6.5 4.8 copy-start.22
  6.5 17.2 %all-gather.11.cloned.1.call-start = ((), (), s32[]{:S(2)}) async-start(), calls=%async_computation.1 | async-start | bytes 4718592 | tf_op jit(solution)/shard_map/all_gather | solution.py:138
  7.3 60.1 %all-gather.17.cloned.1.call-start = ((), (), s32[]{:S(2)}) async-start(), calls=%async_computation.4 | async-start | bytes 1179648 | tf_op jit(solution)/shard_map/all_gather | solution.py:147
  8.0 100.5 %all-gather.19.cloned.1.call-start = ((), (), s32[]{:S(2)}) async-start(), calls=%async_computation.5 | async-start | bytes 1179648 | tf_op jit(solution)/shard_map/all_gather | solution.py:144
  8.7 140.8 %all-gather.15.cloned.1.call-start = ((), (), s32[]{:S(2)}) async-start(), calls=%async_computation.3 | async-start | bytes 1179648 | tf_op jit(solution)/shard_map/all_gather | solution.py:143
  9.3 190.0 %all-gather.13.cloned.1.call-start = ((), (), s32[]{:S(2)}) async-start(), calls=%async_computation.2 | async-start | bytes 2359296 | tf_op jit(solution)/shard_map/all_gather | solution.py:145
  9.9 268.0 %all-gather.21.cloned.1.call-start = ((), (), s32[]{:S(2)}) async-start(), calls=%async_computation.6 | async-start | bytes 2359296 | tf_op jit(solution)/shard_map/all_gather | solution.py:146
  10.5 289.4 %all-gather.23.cloned.1.call-start = ((), (), s32[]{:S(2)}) async-start(), calls=%async_computation.7 | async-start | bytes 2359296 | tf_op jit(solution)/shard_map/all_gather | solution.py:162
  11.2 318.4 %all-reduce.4.cloned.1.call-start = ((), (), s32[]{:S(2)}) async-start(), calls=%async_computation.8 | async-start | bytes 6291456 | tf_op jit(solution)/shard_map/psum | solution.py:165
  11.8 55.5 %copy-start.20 = (f32[768,256]{1,0:T(8,128)S(1)}, f32[768,256]{1,0:T(8,128)}, u32[]{:S(2)}) copy-start(f32[768,256]{1,0:T(8,128)} %param.29) | copy-start | bytes 2359300
  11.8 55.5 %copy-start.21 = (f32[256]{0:T(256)S(1)}, f32[256]{0:T(256)}, u32[]{:S(2)}) copy-start(f32[256]{0:T(256)} %param.28) | copy-start | bytes 3076
  26.3 173.0 %copy-start.17 = (f32[768]{0:T(1024)}, f32[768]{0:T(1024)S(1)}, u32[]{:S(2)}) copy-start(f32[768]{0:T(1024)S(1)} %add_rsqrt_fusion.2) | copy-start | bytes 9220
  166.3 3.8 copy-start.6
  166.3 3.8 copy-start.10
  166.3 3.8 copy-start.11
  257.4 3.7 copy-start.9
  275.3 24.6 %copy-start.18 = (f32[768]{0:T(1024)S(1)}, f32[768]{0:T(1024)}, u32[]{:S(2)}) copy-start(f32[768]{0:T(1024)} %copy-done.17) | copy-start | bytes 9220
  275.8 24.1 %copy-start.2 = (bf16[768,2048]{1,0:T(8,128)(2,1)S(1)}, bf16[768,2048]{1,0:T(8,128)(2,1)}, u32[]{:S(2)}) copy-start(bf16[768,2048]{1,0:T(8,128)(2,1)} %all-gather.11.cloned.1.call-done) | copy-start | bytes 9437188
  308.0 123.7 %all-gather.25.cloned.1.call-start = ((), (), s32[]{:S(2)}) async-start(), calls=%async_computation.9 | async-start | bytes 7077888 | tf_op jit(solution)/shard_map/all_gather | solution.py:174
  308.8 221.9 %all-gather.27.cloned.1.call-start = ((), (), s32[]{:S(2)}) async-start(), calls=%async_computation.10 | async-start | bytes 7077888 | tf_op jit(solution)/shard_map/all_gather | solution.py:175
  309.3 321.1 %all-gather.29.cloned.1.call-start = ((), (), s32[]{:S(2)}) async-start(), calls=%async_computation.11 | async-start | bytes 7077888 | tf_op jit(solution)/shard_map/all_gather | solution.py:182
  310.1 338.7 %reduce-scatter.2.cloned.1.call-start = ((), (), s32[]{:S(2)}) async-start(), calls=%async_computation.12 | async-start | bytes 4718592 | tf_op jit(solution)/shard_map/reduce_scatter | solution.py:184
  440.6 90.0 %copy-start.3 = (bf16[768,2048]{1,0:T(8,128)(2,1)S(1)}, bf16[768,2048]{1,0:T(8,128)(2,1)}, u32[]{:S(2)}) copy-start(bf16[768,2048]{1,0:T(8,128)(2,1)} %get-tuple-element.166) | copy-start | bytes 9437188
  (11 other events, 18.6 us)
Sparse Core Ops, SparseCore 0:
  8.9 14.8 all-gather.10
  25.9 41.4 all-gather.16
  69.5 38.9 all-gather.18
  110.5 38.9 all-gather.14
  151.5 47.7 all-gather.12
  201.3 47.6 all-gather.20
  251.0 48.8 all-gather.22
  308.1 21.4 all-reduce.3
  331.8 99.8 all-gather.24
  433.8 96.8 all-gather.26
  532.7 97.6 all-gather.28
  639.6 9.1 reduce-scatter.1
where the time goes:
time: 669 us; the launch traced here: 659 us
  waiting for transfers between devices  465 us (70%)
  matrix products  76 us (11%)
  local copies, waits for them, and re-layouts  58.3 us (9%)
  other arithmetic  45.3 us (7%)
  between operations  14.2 us (2%)
    all_gather x1, waiting for transfers between devices, local(): lax.all_gather(up_linear_weight, 'fs', axis=0, tiled=True)  97 us
    all_gather x1, waiting for transfers between devices, local(): lax.all_gather(up_gating_weight, 'fs', axis=0, tiled=True)  87.2 us
    all_gather x1, waiting for transfers between devices, local(): lax.all_gather(down_projection_weight, 'fs', axis=1, tiled=True)  83.7 us
    all_gather x1, waiting for transfers between devices, local(): lax.all_gather(decay_projection_weight, 'fs', axis=0, tiled=True)  41 us
    all_gather x1, waiting for transfers between devices, local(): lax.all_gather(key_projection_weight, 'fs', axis=0, tiled=True)  35.2 us
    dot_general x6, matrix products, fold_rows(): jnp.dot(source, weight_piece, preferred_element_type=jnp.float32)  32.4 us
    all_gather x1, waiting for transfers between devices, local(): lax.all_gather(query_projection_weight, 'fs', axis=0, tiled=True)  30.1 us
    all_gather x1, waiting for transfers between devices, local(): lax.all_gather(mixer_result_matrix, 'fs', axis=1, tiled=True)  22 us
  transfers between devices with their start and end apart: 12, of which 11 were waited for; matrix products, arithmetic and copies ran while one was open for 23% of the time, Pallas kernels for 0%

commit v1 on v0

--- a/solution.py
+++ b/solution.py
@@ -2,6 +2,7 @@
 import jax.numpy as jnp
 from jax import lax
 from jax.sharding import PartitionSpec as P
+from jax.lax import all_gather
 
 KEY_DIM = 64
 VALUE_DIM = 128
@@ -135,6 +136,11 @@
     depthwise_bias,
     down_projection_weight,
 ):
+
+    def weights_advance(base_x):
+        finding = all_gather(base_x, "fs")
+        return jnp.concatenate(finding, 1)
+
     whole_rows = lax.all_gather(tokens, "tp", axis=1, tiled=True)
     normed = normalize(whole_rows, first_norm_gain)
     mapped_token_matrix = fold_rows(
@@ -178,9 +184,7 @@
     linear_out = upward[0].astype(jnp.bfloat16)
     gated_out = upward[1].astype(jnp.bfloat16)
     hidden = depthwise(linear_out, gated_out, depthwise_taps, depthwise_bias)
-    channel_terms = emit_with(
-        hidden, lax.all_gather(down_projection_weight, "fs", axis=1, tiled=True)
-    )
+    channel_terms = emit_with(hidden, weights_advance(down_projection_weight))
     channel_part = lax.psum_scatter(
         channel_terms.astype(jnp.bfloat16), "tp", scatter_dimension=1, tiled=True
     ).astype(jnp.float32)

time: 669 us -> 686 us (1.025)
  other arithmetic: 45.3 us -> 53.7 us
    reshape x0 -> x1, local copies, waits for them, and re-layouts: none -> 8.64 us  [weights_advance(): return jnp.concatenate(finding, 1)]
  transfers between devices with their start and end apart: 12 -> 12, of which waited for: 11 -> 11; matrix products, arithmetic and copies ran while one was open for 23% -> 22% of each run, Pallas kernels for 0% -> 0%
where the time goes in v1:
time: 686 us; the launch traced here: 676 us
  waiting for transfers between devices  469 us (68%)
  matrix products  73.4 us (11%)
  local copies, waits for them, and re-layouts  65 us (9%)
  other arithmetic  53.7 us (8%)
  between operations  14.2 us (2%)
    all_gather x1, waiting for transfers between devices, local(): lax.all_gather(up_linear_weight, 'fs', axis=0, tiled=True)  97 us
    all_gather x1, waiting for transfers between devices, weights_advance(): finding = all_gather(base_x, 'fs')  88.1 us
    all_gather x1, waiting for transfers between devices, local(): lax.all_gather(up_gating_weight, 'fs', axis=0, tiled=True)  87.2 us
    all_gather x1, waiting for transfers between devices, local(): lax.all_gather(decay_projection_weight, 'fs', axis=0, tiled=True)  41 us
    all_gather x1, waiting for transfers between devices, local(): lax.all_gather(key_projection_weight, 'fs', axis=0, tiled=True)  35.2 us
    dot_general x6, matrix products, fold_rows(): jnp.dot(source, weight_piece, preferred_element_type=jnp.float32)  32.4 us
    all_gather x1, waiting for transfers between devices, local(): lax.all_gather(query_projection_weight, 'fs', axis=0, tiled=True)  30.1 us
    all_gather x1, waiting for transfers between devices, local(): lax.all_gather(mixer_result_matrix, 'fs', axis=1, tiled=True)  22 us
  transfers between devices with their start and end apart: 12, of which 11 were waited for; matrix products, arithmetic and copies ran while one was open for 22% of the time, Pallas kernels for 0%

profile of v1, /device:TPU:0, one launch (start us, length us, event | category | flops | bytes accessed | tf_op | source)
XLA Modules:
  0.0 676.0 jit_solution(11383684760207287242)
XLA Ops:
  11.8 11.9 %all-gather.12.cloned.1.call-done = bf16[768,2048]{1,0:T(8,128)(2,1)} async-done(((bf16[768,1024]{1,0:T(8,128)(2,1)}), bf16[768,2048]{1,0:T(8,128)(2,1)}) %all-gather.12.cloned.1.call-update) | async-done | bytes 3145744 | tf_op jit(solution)/shard_map/all_gather | solution.py:144
  26.3 41.0 %all-gather.18.cloned.1.call-done = bf16[2048,256]{1,0:T(8,128)(2,1)} async-done(((bf16[256,256]{1,0:T(8,128)(2,1)}), bf16[2048,256]{1,0:T(8,128)(2,1)}) %all-gather.18.cloned.1.call-update) | async-done | bytes 1048592 | tf_op jit(solution)/shard_map/all_gather | solution.py:153
  73.4 35.2 %all-gather.20.cloned.1.call-done = bf16[2048,256]{1,0:T(8,128)(2,1)} async-done(((bf16[256,256]{1,0:T(8,128)(2,1)}), bf16[2048,256]{1,0:T(8,128)(2,1)}) %all-gather.20.cloned.1.call-update) | async-done | bytes 1048592 | tf_op jit(solution)/shard_map/all_gather | solution.py:150
  119.4 30.1 %all-gather.16.cloned.1.call-done = bf16[2048,256]{1,0:T(8,128)(2,1)} async-done(((bf16[256,256]{1,0:T(8,128)(2,1)}), bf16[2048,256]{1,0:T(8,128)(2,1)}) %all-gather.16.cloned.1.call-update) | async-done | bytes 1048592 | tf_op jit(solution)/shard_map/all_gather | solution.py:149
  177.7 21.6 %all-gather.14.cloned.1.call-done = bf16[2048,512]{1,0:T(8,128)(2,1)} async-done(((bf16[256,512]{1,0:T(8,128)(2,1)}), bf16[2048,512]{1,0:T(8,128)(2,1)}) %all-gather.14.cloned.1.call-update) | async-done | bytes 2097168 | tf_op jit(solution)/shard_map/all_gather | solution.py:151
  199.3 5.3 convolution_convert_fusion.5
  214.6 8.1 %while.26 = (s32[]{:T(128)}, f32[3,4,64,128]{3,2,1,0:T(8,128)S(1)}, f32[4,3,4,64,128]{4,3,2,0,1:T(8,128)}, f32[4,3,4,64]{3,2,0,1:T(4,128)S(1)}, f32[4,3,4,64,128]{4,3,2,1,0:T(8,128)}, /*index=5*/s32[]{:T(128)}, s32[]{:T(128)}) while((s32[]{:T(128)}, f32[3,4,64,128]{3,2,1,0:T(8,128)S(1)}, f32[4,3,4,64,128]{4,3,2,0,1:T(8,128)}, ...), condition=%wide.region_3.4_spmd.clone, body=%wide.region_2.3_spmd.clone.sunk | while | flops 393219 | bytes 1975904 | solution.py:53
  229.7 10.2 %rev.17 = f32[3,256,4,128]{3,1,2,0:T(8,128)S(1)} reverse(f32[3,256,4,128]{3,1,2,0:T(8,128)} %copy.80), dimensions={1} | reverse | bytes 3145728 | tf_op jit(solution)/shard_map/jit(_flip)/rev | solution.py:73
  239.9 5.3 fusion.11
  246.5 10.9 %while.27 = (s32[]{:T(128)}, f32[3,4,64,128]{3,2,1,0:T(8,128)S(1)}, f32[4,3,4,64,128]{4,3,2,0,1:T(8,128)}, f32[4,3,4,64]{3,2,0,1:T(4,128)}, f32[4,3,4,64,128]{4,3,2,1,0:T(8,128)}, /*index=5*/s32[]{:T(128)}, s32[]{:T(128)}) while((s32[]{:T(128)}, f32[3,4,64,128]{3,2,1,0:T(8,128)S(1)}, f32[4,3,4,64,128]{4,3,2,0,1:T(8,128)}, ...), condition=%wide.region_6.7_spmd.clone, body=%wide.region_5.6_spmd.clone.sunk | while | flops 393219 | bytes 1975904 | solution.py:53
  264.1 10.6 %rev.21 = f32[3,256,4,128]{3,1,2,0:T(8,128)S(1)} reverse(f32[3,256,4,128]{3,1,2,0:T(8,128)} %bitcast.99), dimensions={1} | reverse | bytes 3145728 | tf_op jit(solution)/shard_map/jit(_flip)/rev | solution.py:76
  277.9 22.0 %all-gather.24.cloned.1.call-done = bf16[512,2048]{1,0:T(8,128)(2,1)} async-done(((bf16[512,256]{1,0:T(8,128)(2,1)}), bf16[512,2048]{1,0:T(8,128)(2,1)}) %all-gather.24.cloned.1.call-update) | async-done | bytes 2097168 | tf_op jit(solution)/shard_map/all_gather | solution.py:168
  299.9 8.1 %convolution_convert_fusion = bf16[768,2048]{1,0:T(8,128)(2,1)} fusion(bf16[512,2048]{1,0:T(8,128)(2,1)} %all-gather.24.cloned.1.call-done, f32[96,8,4,128]{3,2,1,0:T(4,128)} %bitcast.105, bf16[2048,512]{1,0:T(8,128)(2,1)} %all-gather.22.cloned.1.call-done, bf16[768,2048]{1,0:T(8,128)(2,1)S(1)} %copy-done.1, f32[2048]{0:T(1024)S(1)} %convert_element_type.115, ...), kind=kOutput, calls=%fused_computation.19 | convolution fusion | flops 3232235520 | bytes 12069888 | tf_op jit(solution)/shard_map/dot_general | solution.py:117
  310.3 19.3 %all-reduce.4.cloned.1.call-done = bf16[768,2048]{1,0:T(8,128)(2,1)} async-done(((bf16[768,2048]{1,0:T(8,128)(2,1)}), bf16[768,2048]{1,0:T(8,128)(2,1)}) %all-reduce.4.cloned.1.call-update) | async-done | bytes 3145744 | tf_op jit(solution)/shard_map/psum | solution.py:171
  329.6 5.1 fusion
  334.7 97.0 %all-gather.26.cloned.1.call-done = bf16[2048,1536]{1,0:T(8,128)(2,1)} async-done(((bf16[256,1536]{1,0:T(8,128)(2,1)}), bf16[2048,1536]{1,0:T(8,128)(2,1)}) %all-gather.26.cloned.1.call-update) | async-done | bytes 6291472 | tf_op jit(solution)/shard_map/all_gather | solution.py:180
  431.7 8.9 %convolution_convert_fusion.2 = bf16[768,1536]{1,0:T(8,128)(2,1)S(1)} fusion(bf16[2048,1536]{1,0:T(8,128)(2,1)} %all-gather.26.cloned.1.call-done, bf16[768,2048]{1,0:T(8,128)(2,1)} %get-tuple-element.166, f32[2048]{0:T(1024)S(1)} %convert_element_type.133, f32[768]{0:T(1024)S(1)} %add_rsqrt_fusion.1), kind=kOutput, calls=%fused_computation.21 | convolution fusion | flops 4839309312 | bytes 11807744 | tf_op jit(solution)/shard_map/dot_general | solution.py:110
  443.5 87.2 %all-gather.28.cloned.1.call-done = bf16[2048,1536]{1,0:T(8,128)(2,1)} async-done(((bf16[256,1536]{1,0:T(8,128)(2,1)}), bf16[2048,1536]{1,0:T(8,128)(2,1)}) %all-gather.28.cloned.1.call-update) | async-done | bytes 6291472 | tf_op jit(solution)/shard_map/all_gather | solution.py:181
  530.7 8.2 %convolution_convert_fusion.1 = bf16[768,1536]{1,0:T(8,128)(2,1)S(1)} fusion(bf16[2048,1536]{1,0:T(8,128)(2,1)} %all-gather.28.cloned.1.call-done, bf16[768,2048]{1,0:T(8,128)(2,1)S(1)} %copy-done.2, f32[2048]{0:T(1024)S(1)} %convert_element_type.133, f32[768]{0:T(1024)S(1)} %add_rsqrt_fusion.1), kind=kOutput, calls=%fused_computation.20 | convolution fusion | flops 4839309312 | bytes 11807744 | tf_op jit(solution)/shard_map/dot_general | solution.py:110
  541.7 88.1 %all-gather.30.cloned.1.call-done = bf16[12288,256]{1,0:T(8,128)(2,1)} async-done(((bf16[1536,256]{1,0:T(8,128)(2,1)}), bf16[12288,256]{1,0:T(8,128)(2,1)}) %all-gather.30.cloned.1.call-update) | async-done | bytes 6291472 | tf_op jit(solution)/shard_map/all_gather | solution.py:141
  629.8 8.6 %copy.99 = bf16[1536,8,256]{0,2,1:T(8,128)(2,1)} copy(bf16[1536,8,256]{2,0,1:T(8,128)(2,1)} %bitcast.96) | data formatting | bytes 12582912 | tf_op jit(solution)/shard_map/reshape | solution.py:142
  638.4 11.5 %multiply_convert_fusion = bf16[3,256,1536]{2,1,0:T(8,128)(2,1)S(1)} fusion(f32[3,256,1536]{2,1,0:T(8,128)} %convert.12, f32[3,256,1536]{2,1,0:T(8,128)} %convert.11, f32[1536]{0:T(1024)S(1)} %get-tuple-element.141, f32[1536]{0:T(1024)S(1)} %get-tuple-element.142, f32[1536]{0:T(1024)S(1)} %get-tuple-element.138, f32[1536]{0:T(1024)S(1)} %get-tuple-element.144, ...), kind=kLoop, calls=%fused_computation.18 | loop fusion | flops 21233664 | bytes 11845632 | tf_op jit(solution)/shard_map/convert_element_type | solution.py:104
  650.0 6.5 convolution_convert_fusion.3
  656.5 9.3 %reduce-scatter.2.cloned.1.call-done = bf16[768,1024]{1,0:T(8,128)(2,1)} async-done(((bf16[768,2048]{1,0:T(8,128)(2,1)}), bf16[768,1024]{1,0:T(8,128)(2,1)}) %reduce-scatter.2.cloned.1.call-update) | async-done | bytes 1572880 | tf_op jit(solution)/shard_map/reduce_scatter | solution.py:188
  (154 shorter events, 110.6 us)
Async XLA Ops:
  6.5 4.8 copy-start.15
  6.5 4.8 copy-start.22
  6.5 17.2 %all-gather.12.cloned.1.call-start = ((), (), s32[]{:S(2)}) async-start(), calls=%async_computation.1 | async-start | bytes 4718592 | tf_op jit(solution)/shard_map/all_gather | solution.py:144
  7.3 60.1 %all-gather.18.cloned.1.call-start = ((), (), s32[]{:S(2)}) async-start(), calls=%async_computation.4 | async-start | bytes 1179648 | tf_op jit(solution)/shard_map/all_gather | solution.py:153
  8.0 100.5 %all-gather.20.cloned.1.call-start = ((), (), s32[]{:S(2)}) async-start(), calls=%async_computation.5 | async-start | bytes 1179648 | tf_op jit(solution)/shard_map/all_gather | solution.py:150
  8.7 140.8 %all-gather.16.cloned.1.call-start = ((), (), s32[]{:S(2)}) async-start(), calls=%async_computation.3 | async-start | bytes 1179648 | tf_op jit(solution)/shard_map/all_gather | solution.py:149
  9.3 190.0 %all-gather.14.cloned.1.call-start = ((), (), s32[]{:S(2)}) async-start(), calls=%async_computation.2 | async-start | bytes 2359296 | tf_op jit(solution)/shard_map/all_gather | solution.py:151
  9.9 268.0 %all-gather.22.cloned.1.call-start = ((), (), s32[]{:S(2)}) async-start(), calls=%async_computation.6 | async-start | bytes 2359296 | tf_op jit(solution)/shard_map/all_gather | solution.py:152
  10.5 289.4 %all-gather.24.cloned.1.call-start = ((), (), s32[]{:S(2)}) async-start(), calls=%async_computation.7 | async-start | bytes 2359296 | tf_op jit(solution)/shard_map/all_gather | solution.py:168
  11.2 318.4 %all-reduce.4.cloned.1.call-start = ((), (), s32[]{:S(2)}) async-start(), calls=%async_computation.8 | async-start | bytes 6291456 | tf_op jit(solution)/shard_map/psum | solution.py:171
  11.8 55.5 %copy-start.20 = (f32[768,256]{1,0:T(8,128)S(1)}, f32[768,256]{1,0:T(8,128)}, u32[]{:S(2)}) copy-start(f32[768,256]{1,0:T(8,128)} %param.29) | copy-start | bytes 2359300
  11.8 55.5 %copy-start.21 = (f32[256]{0:T(256)S(1)}, f32[256]{0:T(256)}, u32[]{:S(2)}) copy-start(f32[256]{0:T(256)} %param.28) | copy-start | bytes 3076
  26.3 173.0 %copy-start.17 = (f32[768]{0:T(1024)}, f32[768]{0:T(1024)S(1)}, u32[]{:S(2)}) copy-start(f32[768]{0:T(1024)S(1)} %add_rsqrt_fusion.2) | copy-start | bytes 9220
  166.3 3.8 copy-start.5
  166.3 3.8 copy-start.10
  166.3 3.8 copy-start.11
  275.3 24.6 %copy-start.18 = (f32[768]{0:T(1024)S(1)}, f32[768]{0:T(1024)}, u32[]{:S(2)}) copy-start(f32[768]{0:T(1024)} %copy-done.17) | copy-start | bytes 9220
  275.8 24.1 %copy-start.1 = (bf16[768,2048]{1,0:T(8,128)(2,1)S(1)}, bf16[768,2048]{1,0:T(8,128)(2,1)}, u32[]{:S(2)}) copy-start(bf16[768,2048]{1,0:T(8,128)(2,1)} %all-gather.12.cloned.1.call-done) | copy-start | bytes 9437188
  308.0 123.7 %all-gather.26.cloned.1.call-start = ((), (), s32[]{:S(2)}) async-start(), calls=%async_computation.9 | async-start | bytes 7077888 | tf_op jit(solution)/shard_map/all_gather | solution.py:180
  308.8 221.9 %all-gather.28.cloned.1.call-start = ((), (), s32[]{:S(2)}) async-start(), calls=%async_computation.10 | async-start | bytes 7077888 | tf_op jit(solution)/shard_map/all_gather | solution.py:181
  309.3 320.4 %all-gather.30.cloned.1.call-start = ((), (), s32[]{:S(2)}) async-start(), calls=%async_computation.12 | async-start | bytes 7077888 | tf_op jit(solution)/shard_map/all_gather | solution.py:141
  310.1 355.7 %reduce-scatter.2.cloned.1.call-start = ((), (), s32[]{:S(2)}) async-start(), calls=%async_computation.11 | async-start | bytes 4718592 | tf_op jit(solution)/shard_map/reduce_scatter | solution.py:188
  440.6 90.0 %copy-start.2 = (bf16[768,2048]{1,0:T(8,128)(2,1)S(1)}, bf16[768,2048]{1,0:T(8,128)(2,1)}, u32[]{:S(2)}) copy-start(bf16[768,2048]{1,0:T(8,128)(2,1)} %get-tuple-element.166) | copy-start | bytes 9437188
  638.4 11.6 %copy-start.6 = (bf16[1536,8,256]{0,2,1:T(8,128)(2,1)S(1)}, bf16[1536,8,256]{0,2,1:T(8,128)(2,1)}, u32[]{:S(2)}) copy-start(bf16[1536,8,256]{0,2,1:T(8,128)(2,1)} %copy.99) | copy-start | bytes 18874372
  (11 other events, 19.7 us)
Sparse Core Ops, SparseCore 0:
  8.9 14.8 all-gather.11
  25.9 41.4 all-gather.17
  69.5 38.9 all-gather.19
  110.5 38.9 all-gather.15
  151.5 47.7 all-gather.13
  201.3 47.6 all-gather.21
  251.0 48.8 all-gather.23
  308.1 21.4 all-reduce.3
  331.8 99.8 all-gather.25
  433.8 96.8 all-gather.27
  532.9 96.8 all-gather.29
  656.6 9.1 reduce-scatter.1
